TPU v7x, 32 devices: a whole 2x2x4 slice. The times are simulated.
32 devices in a mesh: fs: 8 (over z, y), tp: 4 (over x, core).
Axes of the slice: x: 2, y: 2, z: 4, core: 2. Of those that a mesh axis runs over, the one named last changes fastest.
Arguments:
- tokens: bfloat16 [8192, 2048], P('fs'), may hold values from -6 to 6
- norm_gain: float32 [2048], replicated, may hold values from 0.1 to 1.9
- gate_weight: bfloat16 [2048, 4096], P('fs', 'tp'), may hold values from -0.125 to 0.125
- up_weight: bfloat16 [2048, 4096], P('fs', 'tp'), may hold values from -0.125 to 0.125
- down_weight: bfloat16 [4096, 2048], P('tp', 'fs'), may hold values from -2 to 2
- out_gain: float32 [2048], P('tp'), may hold values from 0.1 to 1.9
Outputs:
- result: bfloat16 [8192, 2048], P('fs', 'tp')
All inputs are finite; a program needn't handle non-finite values.
Results may differ from a plain program's by a relative error of at most 0.014.
Values may be sent and summed in bfloat16 or wider, within the bound.
No kernel may reach another device: no remote copies, remote signals or barrier semaphores. Data moves between devices by JAX's collectives and lax.ppermute only.
A program may use at most 64 MiB of HBM per device.

v0:
```python
import jax
import jax.numpy as jnp
from jax import lax
from jax.sharding import PartitionSpec as P

EPSILON = 1e-06


def body(tokens, norm_gain, gate_weight, up_weight, down_weight, out_gain):
    values = tokens.astype(jnp.float32)
    normed = (
        values * lax.rsqrt(jnp.mean(values * values, axis=1, keepdims=True) + EPSILON) * norm_gain
    ).astype(jnp.bfloat16)
    gate_all, up_all = (
        lax.all_gather(gate_weight, "fs", axis=0, tiled=True),
        lax.all_gather(up_weight, "fs", axis=0, tiled=True),
    )
    gate_proj = jnp.dot(normed, gate_all, preferred_element_type=jnp.float32)
    up_proj = jnp.dot(normed, up_all, preferred_element_type=jnp.float32)
    hidden = (jax.nn.silu(gate_proj) * up_proj).astype(jnp.bfloat16)
    partial_value = jnp.dot(
        hidden,
        lax.all_gather(down_weight, "fs", axis=1, tiled=True),
        preferred_element_type=jnp.float32,
    )
    own_width = out_gain.shape[0]
    own_columns = lax.psum_scatter(
        partial_value.astype(jnp.bfloat16), "tp", scatter_dimension=1, tiled=True
    ).astype(jnp.float32)
    squares = lax.psum(jnp.sum(own_columns * own_columns, axis=1), "tp")
    mean_square = squares / (own_width * lax.axis_size("tp"))
    scaled = own_columns * lax.rsqrt(mean_square + EPSILON)[:, None] * out_gain[None, :]
    return scaled.astype(jnp.bfloat16)


def solution(mesh):
    return jax.shard_map(
        body,
        mesh=mesh,
        in_specs=(P("fs", None), P(), P("fs", "tp"), P("fs", "tp"), P("tp", "fs"), P("tp")),
        out_specs=P("fs", "tp"),
        check_vma=False,
    )
```

profile of v0, /device:TPU:0, one launch (start us, length us, event | category | flops | bytes accessed | tf_op | source)
XLA Modules:
  0.0 308.2 jit_solution(11775894596299125198)
XLA Ops:
  6.5 0.0 copy-start.1
  6.5 0.0 all-gather.4.cloned.1.call-start
  6.5 0.7 all-gather.4.cloned.1.call-update
  7.3 0.0 all-gather.6.cloned.1.call-start
  7.3 0.7 all-gather.6.cloned.1.call-update
  8.0 0.0 all-gather.8.cloned.1.call-start
  8.1 0.7 all-gather.8.cloned.1.call-update
  8.7 0.0 reduce-scatter.2.cloned.1.call-start
  8.8 3.1 fusion
  11.9 73.1 %all-gather.4.cloned.1.call-done = bf16[2048,1024]{1,0:T(8,128)(2,1)} async-done(((bf16[256,1024]{1,0:T(8,128)(2,1)}), bf16[2048,1024]{1,0:T(8,128)(2,1)}) %all-gather.4.cloned.1.call-update) | async-done | bytes 4194320 | tf_op jit(solution)/shard_map/all_gather | solution.py:15
  85.0 0.0 copy-done.1
  85.0 10.0 %fusion.7 = f32[1024,1024]{1,0:T(8,128)} fusion(bf16[2048,1024]{1,0:T(8,128)(2,1)} %all-gather.4.cloned.1.call-done, bf16[1024,2048]{1,0:T(8,128)(2,1)} %param.6, f32[2048]{0:T(1024)S(1)} %copy-done.1, f32[1024]{0:T(1024)S(1)} %add_rsqrt_fusion.1), kind=kOutput, calls=%fused_computation.12 | convolution fusion | flops 4303355904 | bytes 12595200 | tf_op jit(solution)/shard_map/dot_general | solution.py:18
  95.0 63.5 %all-gather.6.cloned.1.call-done = bf16[2048,1024]{1,0:T(8,128)(2,1)} async-done(((bf16[256,1024]{1,0:T(8,128)(2,1)}), bf16[2048,1024]{1,0:T(8,128)(2,1)}) %all-gather.6.cloned.1.call-update) | async-done | bytes 4194320 | tf_op jit(solution)/shard_map/all_gather | solution.py:16
  158.5 75.3 %all-gather.8.cloned.1.call-done = bf16[1024,2048]{1,0:T(8,128)(2,1)} async-done(((bf16[1024,256]{1,0:T(8,128)(2,1)}), bf16[1024,2048]{1,0:T(8,128)(2,1)}) %all-gather.8.cloned.1.call-update) | async-done | bytes 4194320 | tf_op jit(solution)/shard_map/all_gather | solution.py:23
  233.7 15.3 %convolution_convert_fusion = bf16[1024,2048]{1,0:T(8,128)(2,1)} fusion(bf16[1024,2048]{1,0:T(8,128)(2,1)} %all-gather.8.cloned.1.call-done, f32[1024,1024]{1,0:T(8,128)} %fusion.7, bf16[2048,1024]{1,0:T(8,128)(2,1)} %all-gather.6.cloned.1.call-done, bf16[1024,2048]{1,0:T(8,128)(2,1)} %param.6, f32[2048]{0:T(1024)S(1)} %copy-done.1, ...), kind=kOutput, calls=%fused_computation.6 | convolution fusion | flops 8606711808 | bytes 20983808 | tf_op jit(solution)/shard_map/dot_general | solution.py:21
  249.1 0.0 copy-start
  249.1 0.0 reduce-scatter.2.cloned.1.call-update
  249.1 42.7 %reduce-scatter.2.cloned.1.call-done = bf16[1024,512]{1,0:T(8,128)(2,1)} async-done(((bf16[1024,2048]{1,0:T(8,128)(2,1)}), bf16[1024,512]{1,0:T(8,128)(2,1)}) %reduce-scatter.2.cloned.1.call-update) | async-done | bytes 1048592 | tf_op jit(solution)/shard_map/reduce_scatter | solution.py:27
  291.9 1.5 fusion.3
  293.4 5.8 %psum.7 = f32[1024]{0:T(1024)S(1)} all-reduce(f32[1024]{0:T(1024)S(1)} %fusion.3), channel_id=1, replica_groups=mesh['fs'=8,'tp'=4] {'tp'}, use_global_device_ids=true, to_apply=%region_3.4 | all-reduce | flops 1024 | bytes 8192 | tf_op jit(solution)/shard_map/psum | solution.py:30
  299.1 0.0 copy-done
  299.1 2.5 fusion.5
  (2 shorter events, 0.0 us)
Async XLA Ops:
  6.5 78.5 %copy-start.1 = (f32[2048]{0:T(1024)S(1)}, f32[2048]{0:T(1024)}, u32[]{:S(2)}) copy-start(f32[2048]{0:T(1024)} %param.7) | copy-start | bytes 24580
  6.5 78.5 %all-gather.4.cloned.1.call-start = ((), (), s32[]{:S(2)}) async-start(), calls=%async_computation.1 | async-start | bytes 4718592 | tf_op jit(solution)/shard_map/all_gather | solution.py:15
  7.3 151.2 %all-gather.6.cloned.1.call-start = ((), (), s32[]{:S(2)}) async-start(), calls=%async_computation.2 | async-start | bytes 4718592 | tf_op jit(solution)/shard_map/all_gather | solution.py:16
  8.0 225.7 %all-gather.8.cloned.1.call-start = ((), (), s32[]{:S(2)}) async-start(), calls=%async_computation.3 | async-start | bytes 4718592 | tf_op jit(solution)/shard_map/all_gather | solution.py:23
  8.7 283.1 %reduce-scatter.2.cloned.1.call-start = ((), (), s32[]{:S(2)}) async-start(), calls=%async_computation.4 | async-start | bytes 5242880 | tf_op jit(solution)/shard_map/reduce_scatter | solution.py:27
  249.1 50.0 %copy-start = (f32[512]{0:T(512)S(1)}, f32[512]{0:T(512)}, u32[]{:S(2)}) copy-start(f32[512]{0:T(512)} %param.11) | copy-start | bytes 6148
Sparse Core Ops, SparseCore 0:
  9.5 75.5 all-gather.3
  87.1 71.3 all-gather.5
  160.5 73.1 all-gather.7
  249.2 42.5 reduce-scatter.1
where the time goes:
time: 308 us
  waiting for transfers between devices  257 us (83%)
  matrix products  25.3 us (8%)
  between operations  13.1 us (4%)
  other arithmetic  7.09 us (2%)
  blocking collectives  5.77 us (2%)
    all_gather x1, waiting for transfers between devices, body(): lax.all_gather(down_weight, 'fs', axis=1, tiled=True)  75.3 us
    all_gather x1, waiting for transfers between devices, body(): lax.all_gather(gate_weight, 'fs', axis=0, tiled=True)  73.1 us
    all_gather x1, waiting for transfers between devices, body(): lax.all_gather(up_weight, 'fs', axis=0, tiled=True)  63.5 us
    reduce_scatter x1, waiting for transfers between devices, body(): lax.psum_scatter(partial_value.astype(jnp.bfloat16), 'tp', scatter_dimens...  42.7 us
    dot_general x1, matrix products, body(): jnp.dot(hidden, lax.all_gather(down_weight, 'fs', axis=1, tiled=True), pr...  15.3 us
    dot_general x1, matrix products, body(): gate_proj = jnp.dot(normed, gate_all, preferred_element_type=jnp.float32)  9.96 us
  transfers between devices with their start and end apart: 4, of which 4 were waited for; matrix products, arithmetic and copies ran while one was open for 4% of the time, Pallas kernels for 0%

commit v1 on v0

--- a/solution.py
+++ b/solution.py
@@ -6,13 +6,35 @@
 EPSILON = 1e-06
 
 
+def joined_along(blocks, dim):
+    blocks = jnp.moveaxis(blocks, 0, dim)
+    shape = blocks.shape
+    return blocks.reshape(*shape[:dim], shape[dim] * shape[dim + 1], *shape[dim + 2 :])
+
+
+def ring_gather(shard, axis, dim):
+    size = lax.axis_size(axis)
+    pairs = [(i, (i + 1) % size) for i in range(size)]
+    back = [(b, a) for a, b in pairs]
+    lower, upper = ([], [])
+    for step in range(size - 1):
+        if step % 2 == 0:
+            lower.append(lax.ppermute(lower[-1] if lower else shard, axis, pairs))
+        else:
+            upper.append(lax.ppermute(upper[-1] if upper else shard, axis, back))
+    parts = jnp.stack([*lower[::-1], shard, *upper])
+    shift = lax.axis_index(axis) - len(lower)
+    parts = parts[(jnp.arange(size) - shift) % size]
+    return joined_along(parts, dim)
+
+
 def body(tokens, norm_gain, gate_weight, up_weight, down_weight, out_gain):
     values = tokens.astype(jnp.float32)
     normed = (
         values * lax.rsqrt(jnp.mean(values * values, axis=1, keepdims=True) + EPSILON) * norm_gain
     ).astype(jnp.bfloat16)
     gate_all, up_all = (
-        lax.all_gather(gate_weight, "fs", axis=0, tiled=True),
+        ring_gather(gate_weight, "fs", 0),
         lax.all_gather(up_weight, "fs", axis=0, tiled=True),
     )
     gate_proj = jnp.dot(normed, gate_all, preferred_element_type=jnp.float32)

time: 308 us -> 287 us (0.932)
  waiting for transfers between devices: 257 us -> 198 us
  starting transfers between devices: 0.12 us -> 25.3 us
  local copies, waits for them, and re-layouts: 0.01 us -> 11.7 us
    ppermute x0 -> x7, waiting for transfers between devices: none -> 83.9 us  [the longest x4 83.9 us: ring_gather(): lower.append(lax.ppermute(lower[-1] if lower else shard, axis, pairs))]
    all_gather x1 -> x0, waiting for transfers between devices: 73.1 us -> none  [body(): lax.all_gather(gate_weight, 'fs', axis=0, tiled=True)]
    all_gather x1, waiting for transfers between devices: 63.5 us -> 3.91 us  [body(): lax.all_gather(up_weight, 'fs', axis=0, tiled=True)]
    ppermute x0 -> x7, starting transfers between devices: none -> 25.2 us  [the longest x3 18.7 us: ring_gather(): upper.append(lax.ppermute(upper[-1] if upper else shard, axis, back))]
    all_gather x1, waiting for transfers between devices: 75.3 us -> 65.8 us  [body(): lax.all_gather(down_weight, 'fs', axis=1, tiled=True)]
    unnamed x4 -> x13, local copies, waits for them, and re-layouts: 0.01 us -> 5.86 us
    gather x0 -> x1, local copies, waits for them, and re-layouts: none -> 4.98 us  [ring_gather(): parts = parts[(jnp.arange(size) - shift) % size]]
  transfers between devices with their start and end apart: 4 -> 10, of which waited for: 4 -> 7; matrix products, arithmetic and copies ran while one was open for 4% -> 9% of each run, Pallas kernels for 0% -> 0%
where the time goes in v1:
time: 287 us; the launch traced here: 286 us
  waiting for transfers between devices  198 us (69%)
  matrix products  25.6 us (9%)
  starting transfers between devices  25.3 us (9%)
  between operations  13.2 us (5%)
  local copies, waits for them, and re-layouts  11.7 us (4%)
  other arithmetic  7.16 us (2%)
  blocking collectives  5.77 us (2%)
    ppermute x4, waiting for transfers between devices, ring_gather(): lower.append(lax.ppermute(lower[-1] if lower else shard, axis, pairs))  83.9 us
    all_gather x1, waiting for transfers between devices, body(): lax.all_gather(down_weight, 'fs', axis=1, tiled=True)  65.8 us
    reduce_scatter x1, waiting for transfers between devices, body(): lax.psum_scatter(partial_value.astype(jnp.bfloat16), 'tp', scatter_dimens...  42.7 us
    ppermute x3, starting transfers between devices, ring_gather(): upper.append(lax.ppermute(upper[-1] if upper else shard, axis, back))  18.7 us
    dot_general x1, matrix products, body(): jnp.dot(hidden, lax.all_gather(down_weight, 'fs', axis=1, tiled=True), pr...  15.7 us
    dot_general x1, matrix products, body(): up_proj = jnp.dot(normed, up_all, preferred_element_type=jnp.float32)  9.95 us
    ppermute x4, starting transfers between devices, ring_gather(): lower.append(lax.ppermute(lower[-1] if lower else shard, axis, pairs))  6.49 us
    unnamed x13, local copies, waits for them, and re-layouts  5.86 us
  transfers between devices with their start and end apart: 10, of which 7 were waited for; matrix products, arithmetic and copies ran while one was open for 9% of the time, Pallas kernels for 0%

profile of v1, /device:TPU:0, one launch (start us, length us, event | category | flops | bytes accessed | tf_op | source)
XLA Modules:
  0.0 286.5 jit_solution(4316126266696337796)
XLA Ops:
  8.1 3.0 %collective-permute-start = (bf16[256,1024]{1,0:T(8,128)(2,1)}, bf16[256,1024]{1,0:T(8,128)(2,1)S(1)}, u32[]{:S(2)}, u32[]{:S(2)}) collective-permute-start(bf16[256,1024]{1,0:T(8,128)(2,1)} %param.8), channel_id=1, source_target_pairs={{0,4},{4,8},{8,12},{12,16},{16,20},{20,24},{24,28},{28,0},{1,5},{5... | collective-permute-start | bytes 1572872 | tf_op jit(solution)/shard_map/ppermute | solution.py:22
  11.1 15.7 %collective-permute-done = bf16[256,1024]{1,0:T(8,128)(2,1)S(1)} collective-permute-done((bf16[256,1024]{1,0:T(8,128)(2,1)}, bf16[256,1024]{1,0:T(8,128)(2,1)S(1)}, u32[]{:S(2)}, u32[]{:S(2)}) %collective-permute-start) | collective-permute-done | bytes 524320 | tf_op jit(solution)/shard_map/ppermute | solution.py:22
  26.8 1.0 collective-permute-start.1
  27.8 3.8 %collective-permute-start.4 = (bf16[256,1024]{1,0:T(8,128)(2,1)}, bf16[256,1024]{1,0:T(8,128)(2,1)S(1)}, u32[]{:S(2)}, u32[]{:S(2)}) collective-permute-start(bf16[256,1024]{1,0:T(8,128)(2,1)} %param.8), channel_id=1, source_target_pairs={{4,0},{8,4},{12,8},{16,12},{20,16},{24,20},{28,24},{0,28},{5,1},{9... | collective-permute-start | bytes 1572872 | tf_op jit(solution)/shard_map/ppermute | solution.py:24
  31.5 22.9 %collective-permute-done.1 = bf16[256,1024]{1,0:T(8,128)(2,1)S(1)} collective-permute-done((bf16[256,1024]{1,0:T(8,128)(2,1)S(1)}, bf16[256,1024]{1,0:T(8,128)(2,1)S(1)}, u32[]{:S(2)}, u32[]{:S(2)}) %collective-permute-start.1) | collective-permute-done | bytes 524320 | tf_op jit(solution)/shard_map/ppermute | solution.py:22
  54.5 4.8 %collective-permute-start.5 = (bf16[256,1024]{1,0:T(8,128)(2,1)S(1)}, bf16[256,1024]{1,0:T(8,128)(2,1)S(1)}, u32[]{:S(2)}, u32[]{:S(2)}) collective-permute-start(bf16[256,1024]{1,0:T(8,128)(2,1)S(1)} %collective-permute-done.4), channel_id=1, source_target_pairs={{4,0},{8,4},{12,8},{16,12},{20,16},{24,20},{28,24},{0,28},{5,1},{9... | collective-permute-start | bytes 1572872 | tf_op jit(solution)/shard_map/ppermute | solution.py:24
  59.2 27.4 %collective-permute-done.2 = bf16[256,1024]{1,0:T(8,128)(2,1)S(1)} collective-permute-done((bf16[256,1024]{1,0:T(8,128)(2,1)S(1)}, bf16[256,1024]{1,0:T(8,128)(2,1)S(1)}, u32[]{:S(2)}, u32[]{:S(2)}) %collective-permute-start.2) | collective-permute-done | bytes 524320 | tf_op jit(solution)/shard_map/ppermute | solution.py:22
  86.7 2.5 collective-permute-start.3
  89.1 3.1 %fusion = f32[1024]{0:T(1024)S(1)} fusion(bf16[1024,2048]{1,0:T(8,128)(2,1)} %param.6), kind=kLoop, calls=%fused_computation.3 | loop fusion | flops 6290432 | bytes 4198400 | tf_op jit(solution)/shard_map/reduce_sum | solution.py:34
  92.3 10.2 %collective-permute-start.6 = (bf16[256,1024]{1,0:T(8,128)(2,1)S(1)}, bf16[256,1024]{1,0:T(8,128)(2,1)S(1)}, u32[]{:S(2)}, u32[]{:S(2)}) collective-permute-start(bf16[256,1024]{1,0:T(8,128)(2,1)S(1)} %collective-permute-done.5), channel_id=1, source_target_pairs={{4,0},{8,4},{12,8},{16,12},{20,16},{24,20},{28,24},{0,28},{5,1},{9... | collective-permute-start | bytes 1572872 | tf_op jit(solution)/shard_map/ppermute | solution.py:24
  102.5 17.9 %collective-permute-done.3 = bf16[256,1024]{1,0:T(8,128)(2,1)S(1)} collective-permute-done((bf16[256,1024]{1,0:T(8,128)(2,1)S(1)}, bf16[256,1024]{1,0:T(8,128)(2,1)S(1)}, u32[]{:S(2)}, u32[]{:S(2)}) %collective-permute-start.3) | collective-permute-done | bytes 524320 | tf_op jit(solution)/shard_map/ppermute | solution.py:22
  120.4 0.9 bitcast_dynamic-update-slice_fusion.7
  121.2 0.9 bitcast_dynamic-update-slice_fusion.6
  123.7 0.8 bitcast_dynamic-update-slice_fusion.3
  126.2 0.8 bitcast_dynamic-update-slice_fusion
  127.1 5.0 %gather_fusion = bf16[8,256,1024]{2,1,0:T(8,128)(2,1)} fusion(bf16[8,256,1024]{2,1,0:T(8,128)(2,1)} %bitcast_dynamic-update-slice_fusion, s32[1024]{0:T(1024)S(1)} %pad_clamp_fusion), kind=kCustom, calls=%fused_computation | custom fusion | bytes 8388640 | tf_op jit(solution)/shard_map/gather | solution.py:27
  132.0 3.9 %all-gather.3.cloned.1.call-done = bf16[2048,1024]{1,0:T(8,128)(2,1)} async-done(((bf16[256,1024]{1,0:T(8,128)(2,1)}), bf16[2048,1024]{1,0:T(8,128)(2,1)}) %all-gather.3.cloned.1.call-update) | async-done | bytes 4194320 | tf_op jit(solution)/shard_map/all_gather | solution.py:38
  136.0 9.9 %fusion.7 = f32[1024,1024]{1,0:T(8,128)} fusion(bf16[2048,1024]{1,0:T(8,128)(2,1)} %all-gather.3.cloned.1.call-done, bf16[1024,2048]{1,0:T(8,128)(2,1)} %param.6, f32[2048]{0:T(1024)S(1)} %copy-done.2, f32[1024]{0:T(1024)S(1)} %add_rsqrt_fusion.1), kind=kOutput, calls=%fused_computation.14 | convolution fusion | flops 4303355904 | bytes 12595200 | tf_op jit(solution)/shard_map/dot_general | solution.py:41
  145.9 65.8 %all-gather.5.cloned.1.call-done = bf16[1024,2048]{1,0:T(8,128)(2,1)} async-done(((bf16[1024,256]{1,0:T(8,128)(2,1)}), bf16[1024,2048]{1,0:T(8,128)(2,1)}) %all-gather.5.cloned.1.call-update) | async-done | bytes 4194320 | tf_op jit(solution)/shard_map/all_gather | solution.py:45
  211.7 15.7 %convolution_convert_fusion = bf16[1024,2048]{1,0:T(8,128)(2,1)} fusion(bf16[1024,2048]{1,0:T(8,128)(2,1)} %all-gather.5.cloned.1.call-done, f32[1024,1024]{1,0:T(8,128)} %fusion.7, bf16[2048,1024]{1,0:T(8,128)(2,1)} %bitcast.22, bf16[1024,2048]{1,0:T(8,128)(2,1)} %param.6, f32[2048]{0:T(1024)S(1)} %copy-done.2, f32[1024]{0:T(1024)S(1)} %add_rsqrt_fusion.1), kind=kOutput, calls=%fused_computation.7 | convolution fusion | flops 8606711808 | bytes 20983808 | tf_op jit(solution)/shard_map/dot_general | solution.py:43
  227.4 42.7 %reduce-scatter.2.cloned.1.call-done = bf16[1024,512]{1,0:T(8,128)(2,1)} async-done(((bf16[1024,2048]{1,0:T(8,128)(2,1)}), bf16[1024,512]{1,0:T(8,128)(2,1)}) %reduce-scatter.2.cloned.1.call-update) | async-done | bytes 1048592 | tf_op jit(solution)/shard_map/reduce_scatter | solution.py:49
  270.2 1.5 fusion.3
  271.7 5.8 %psum.7 = f32[1024]{0:T(1024)S(1)} all-reduce(f32[1024]{0:T(1024)S(1)} %fusion.3), channel_id=1, replica_groups=mesh['fs'=8,'tp'=4] {'tp'}, use_global_device_ids=true, to_apply=%region_3.4 | all-reduce | flops 1024 | bytes 8192 | tf_op jit(solution)/shard_map/psum | solution.py:52
  277.5 2.5 fusion.5
  (24 shorter events, 4.9 us)
Async XLA Ops:
  6.5 129.4 %all-gather.3.cloned.1.call-start = ((), (), s32[]{:S(2)}) async-start(), calls=%async_computation.1 | async-start | bytes 4718592 | tf_op jit(solution)/shard_map/all_gather | solution.py:38
  7.3 204.5 %all-gather.5.cloned.1.call-start = ((), (), s32[]{:S(2)}) async-start(), calls=%async_computation.2 | async-start | bytes 4718592 | tf_op jit(solution)/shard_map/all_gather | solution.py:45
  8.0 262.2 %reduce-scatter.2.cloned.1.call-start = ((), (), s32[]{:S(2)}) async-start(), calls=%async_computation.3 | async-start | bytes 5242880 | tf_op jit(solution)/shard_map/reduce_scatter | solution.py:49
  8.1 18.8 %collective-permute-start = (bf16[256,1024]{1,0:T(8,128)(2,1)}, bf16[256,1024]{1,0:T(8,128)(2,1)S(1)}, u32[]{:S(2)}, u32[]{:S(2)}) collective-permute-start(bf16[256,1024]{1,0:T(8,128)(2,1)} %param.8), channel_id=1, source_target_pairs={{0,4},{4,8},{8,12},{12,16},{16,20},{20,24},{24,28},{28,0},{1,5},{5... | collective-permute-start | bytes 1572872 | tf_op jit(solution)/shard_map/ppermute | solution.py:22
  26.8 27.6 %collective-permute-start.1 = (bf16[256,1024]{1,0:T(8,128)(2,1)S(1)}, bf16[256,1024]{1,0:T(8,128)(2,1)S(1)}, u32[]{:S(2)}, u32[]{:S(2)}) collective-permute-start(bf16[256,1024]{1,0:T(8,128)(2,1)S(1)} %collective-permute-done), channel_id=1, source_target_pairs={{0,4},{4,8},{8,12},{12,16},{16,20},{20,24},{24,28},{28,0},{1,5},{5... | collective-permute-start | bytes 1572872 | tf_op jit(solution)/shard_map/ppermute | solution.py:22
  27.8 26.7 %collective-permute-start.4 = (bf16[256,1024]{1,0:T(8,128)(2,1)}, bf16[256,1024]{1,0:T(8,128)(2,1)S(1)}, u32[]{:S(2)}, u32[]{:S(2)}) collective-permute-start(bf16[256,1024]{1,0:T(8,128)(2,1)} %param.8), channel_id=1, source_target_pairs={{4,0},{8,4},{12,8},{16,12},{20,16},{24,20},{28,24},{0,28},{5,1},{9... | collective-permute-start | bytes 1572872 | tf_op jit(solution)/shard_map/ppermute | solution.py:24
  54.4 32.2 %collective-permute-start.2 = (bf16[256,1024]{1,0:T(8,128)(2,1)S(1)}, bf16[256,1024]{1,0:T(8,128)(2,1)S(1)}, u32[]{:S(2)}, u32[]{:S(2)}) collective-permute-start(bf16[256,1024]{1,0:T(8,128)(2,1)S(1)} %collective-permute-done.1), channel_id=1, source_target_pairs={{0,4},{4,8},{8,12},{12,16},{16,20},{20,24},{24,28},{28,0},{1,5},{5... | collective-permute-start | bytes 1572872 | tf_op jit(solution)/shard_map/ppermute | solution.py:22
  54.4 69.3 %copy-start = (bf16[256,1024]{1,0:T(8,128)(2,1)S(1)}, bf16[256,1024]{1,0:T(8,128)(2,1)}, u32[]{:S(2)}) copy-start(bf16[256,1024]{1,0:T(8,128)(2,1)} %param.8) | copy-start | bytes 1572868
  54.5 37.8 %collective-permute-start.5 = (bf16[256,1024]{1,0:T(8,128)(2,1)S(1)}, bf16[256,1024]{1,0:T(8,128)(2,1)S(1)}, u32[]{:S(2)}, u32[]{:S(2)}) collective-permute-start(bf16[256,1024]{1,0:T(8,128)(2,1)S(1)} %collective-permute-done.4), channel_id=1, source_target_pairs={{4,0},{8,4},{12,8},{16,12},{20,16},{24,20},{28,24},{0,28},{5,1},{9... | collective-permute-start | bytes 1572872 | tf_op jit(solution)/shard_map/ppermute | solution.py:24
  86.7 33.7 %collective-permute-start.3 = (bf16[256,1024]{1,0:T(8,128)(2,1)S(1)}, bf16[256,1024]{1,0:T(8,128)(2,1)S(1)}, u32[]{:S(2)}, u32[]{:S(2)}) collective-permute-start(bf16[256,1024]{1,0:T(8,128)(2,1)S(1)} %collective-permute-done.2), channel_id=1, source_target_pairs={{0,4},{4,8},{8,12},{12,16},{16,20},{20,24},{24,28},{28,0},{1,5},{5... | collective-permute-start | bytes 1572872 | tf_op jit(solution)/shard_map/ppermute | solution.py:22
  92.3 34.0 %collective-permute-start.6 = (bf16[256,1024]{1,0:T(8,128)(2,1)S(1)}, bf16[256,1024]{1,0:T(8,128)(2,1)S(1)}, u32[]{:S(2)}, u32[]{:S(2)}) collective-permute-start(bf16[256,1024]{1,0:T(8,128)(2,1)S(1)} %collective-permute-done.5), channel_id=1, source_target_pairs={{4,0},{8,4},{12,8},{16,12},{20,16},{24,20},{28,24},{0,28},{5,1},{9... | collective-permute-start | bytes 1572872 | tf_op jit(solution)/shard_map/ppermute | solution.py:24
  127.1 8.9 %copy-start.2 = (f32[2048]{0:T(1024)S(1)}, f32[2048]{0:T(1024)}, u32[]{:S(2)}) copy-start(f32[2048]{0:T(1024)} %param.7) | copy-start | bytes 24580
  227.4 50.0 %copy-start.1 = (f32[512]{0:T(512)S(1)}, f32[512]{0:T(512)}, u32[]{:S(2)}) copy-start(f32[512]{0:T(512)} %param.11) | copy-start | bytes 6148
Sparse Core Ops, SparseCore 0:
  9.5 126.4 all-gather.2
  138.0 73.6 all-gather.4
  227.6 42.5 reduce-scatter.1
